TPU v7x, 32 devices: a whole 2x2x4 slice. The times are simulated.
32 devices in a mesh: grp: 2 (over y), sp: 8 (over z, core), tp: 2 (over x).
Axes of the slice: x: 2, y: 2, z: 4, core: 2. Of those that a mesh axis runs over, the one named last changes fastest.
Arguments:
- queries_a: bfloat16 [4096, 2, 512], P(('grp', 'sp'), None, 'tp'), parts along dimension 0, may hold values from -120 to 120
- keys_a: bfloat16 [4096, 2, 512], P(('grp', 'sp'), None, 'tp'), parts along dimension 0, may hold values from -6 to 6
- values_a: bfloat16 [4096, 1024], P(('grp', 'sp'), 'tp'), parts along dimension 0, may hold values from -6 to 6
- queries_b: bfloat16 [4096, 2, 512], P(('grp', 'sp'), None, 'tp'), parts along dimension 0, may hold values from -120 to 120
- keys_b: bfloat16 [4096, 2, 512], P(('grp', 'sp'), None, 'tp'), parts along dimension 0, may hold values from -6 to 6
- values_b: bfloat16 [4096, 1024], P(('grp', 'sp'), 'tp'), parts along dimension 0, may hold values from -6 to 6
- lambdas: float32 [12], replicated, may hold values from 0.3 to 0.8
- head_gain_a: float32 [256], replicated, may hold values from 0.1 to 1.9
- head_gain_b: float32 [128], replicated, may hold values from 0.1 to 1.9
- out_a: bfloat16 [1024, 2048], P('tp'), may hold values from -0.125 to 0.125
- out_b: bfloat16 [1024, 2048], P('tp'), may hold values from -0.125 to 0.125
- residual: bfloat16 [4096, 2048], P(('grp', 'sp', 'tp')), parts along dimension 0, may hold values from -6 to 6
- gain_mix: float32 [2048], replicated, may hold values from 0.1 to 1.9
- gain_pre: float32 [2048], replicated, may hold values from 0.1 to 1.9
- gain_post: float32 [2048], replicated, may hold values from 0.1 to 1.9
- routes: int32 [4096, 4], P(('grp', 'sp', 'tp')), parts along dimension 0, may hold values from 0 to 7, all different within a row; in each aligned block of 128 rows (0 to 127, 128 to 255, ...) at most 80 rows name the same one
- route_weights: float32 [4096, 4], P(('grp', 'sp', 'tp')), parts along dimension 0, may hold values from 0.05 to 1
- expert_gate: bfloat16 [8, 2048, 2048], P('sp', None, 'tp'), may hold values from -1 to 1
- expert_up: bfloat16 [8, 2048, 2048], P('sp', None, 'tp'), may hold values from -1 to 1
- expert_down: bfloat16 [8, 2048, 2048], P('sp', 'tp'), may hold values from -0.125 to 0.125
Outputs:
- layer_out: bfloat16 [4096, 2048], P(('grp', 'sp', 'tp')), parts along dimension 0
There are 2 independent parts, one for each index of `grp`. A program takes and returns all parts, laid end to end along the dimension named above; an argument that names none is the same for every part. Nothing has to cross between parts.
Inputs may be any that keep to these rules, and one draw needn't show every extreme that they name: `routes`: in each aligned block of 128 rows (the rows of one device) no expert is named by more than 80 rows, a bound that some blocks reach.
All inputs are finite; a program needn't handle non-finite values.
Results may differ from a plain program's by a relative error of at most 0.018.
Values may be sent and summed in bfloat16 or wider, within the bound.
A program may use at most 128 MiB of HBM per device.

v0:
```python
import jax
import jax.numpy as jnp
from jax import lax
from jax.sharding import PartitionSpec as P

HA = 4
DA = 128
DB = 64


def rms_norm(values, gain_vec):
    return values * lax.rsqrt(jnp.mean(values * values, -1, keepdims=True) + 1e-06) * gain_vec


def attend(current, query_rows, key_rows, value_rows, first_row, query_pos, head_size):
    run_max, run_sum, run_acc = current
    key_count = key_rows.shape[0]
    heads = query_rows.shape[2]
    key_view = key_rows.reshape(key_count, 2, heads, head_size)
    value_view = value_rows.reshape(key_count, heads, 2 * head_size)
    key_pos = first_row + jnp.arange(key_count, dtype=jnp.int32)
    visible = (key_pos[None, :] <= query_pos[:, None])[None, :, None, :]
    scores = jnp.einsum(
        "qmhd,kmhd->mqhk", query_rows, key_view, preferred_element_type=jnp.float32
    ) * head_size ** (-0.5)
    scores = jnp.where(visible, scores, -1e30)
    new_max = jnp.maximum(run_max, jnp.max(scores, -1))
    exp_terms = jnp.where(visible, jnp.exp(scores - new_max[..., None]), 0.0)
    rescale = jnp.exp(run_max - new_max)
    run_sum = run_sum * rescale + jnp.sum(exp_terms, -1)
    run_acc = run_acc * rescale[..., None] + jnp.einsum(
        "mqhk,khe->mqhe",
        exp_terms.astype(jnp.bfloat16),
        value_view,
        preferred_element_type=jnp.float32,
    )
    return (new_max, run_sum, run_acc)


def fresh_state(length, heads, head_size):
    return (
        jnp.full((2, length, heads), -1e30, jnp.float32),
        jnp.zeros((2, length, heads), jnp.float32),
        jnp.zeros((2, length, heads, 2 * head_size), jnp.float32),
    )


def finish(current, weights_two, gain_vec):
    run_max, run_sum, run_acc = current
    mixture = (
        run_acc[0] / run_sum[0][..., None]
        - weights_two[None, :, None] * run_acc[1] / run_sum[1][..., None]
    )
    normed = rms_norm(mixture, gain_vec)
    return normed.reshape(normed.shape[0], -1).astype(jnp.bfloat16)


def slot_numbers(flat_ids, experts):
    onehot = (flat_ids[:, None] == jnp.arange(experts, dtype=jnp.int32)[None, :]).astype(jnp.int32)
    before = jnp.cumsum(onehot, 0) - onehot
    return jnp.sum(before * onehot, 1)


def send_matrix(route_rows, experts, capacity):
    groups, sub_rows, top_count = route_rows.shape
    slot_ids = jax.vmap(lambda flat_ids: slot_numbers(flat_ids, experts))(
        route_rows.reshape(groups, -1)
    )
    group_ids = jnp.arange(groups, dtype=jnp.int32)[:, None]
    row_ids = (
        route_rows.reshape(groups, -1) * (groups * capacity) + group_ids * capacity + slot_ids
    ).reshape(-1)
    col_ids = jnp.broadcast_to(
        group_ids[:, :, None] * sub_rows + jnp.arange(sub_rows, dtype=jnp.int32)[None, :, None],
        route_rows.shape,
    ).reshape(-1)
    row_hot = (
        row_ids[:, None] == jnp.arange(experts * groups * capacity, dtype=jnp.int32)[None, :]
    ).astype(jnp.bfloat16)
    col_hot = (col_ids[:, None] == jnp.arange(groups * sub_rows, dtype=jnp.int32)[None, :]).astype(
        jnp.bfloat16
    )
    return jnp.einsum("ar,ac->rc", row_hot, col_hot, preferred_element_type=jnp.float32).astype(
        jnp.bfloat16
    )


def back_matrix(route_rows, route_weights, experts, capacity):
    sub_rows, top_count = route_rows.shape
    slot_ids = slot_numbers(route_rows.reshape(-1), experts)
    row_ids = route_rows.reshape(-1) * capacity + slot_ids
    col_ids = jnp.repeat(jnp.arange(sub_rows, dtype=jnp.int32), top_count)
    row_hot = (row_ids[:, None] == jnp.arange(experts * capacity, dtype=jnp.int32)[None, :]).astype(
        jnp.float32
    )
    tok_weighted = (col_ids[:, None] == jnp.arange(sub_rows, dtype=jnp.int32)[None, :]).astype(
        jnp.float32
    ) * route_weights.reshape(-1)[:, None]
    return jnp.einsum("at,ar->tr", tok_weighted, row_hot, precision=lax.Precision.HIGHEST)


def per_device(
    queries_a,
    keys_a,
    values_a,
    queries_b,
    keys_b,
    values_b,
    lambdas,
    head_gain_a,
    head_gain_b,
    out_a,
    out_b,
    residual,
    gain_mix,
    gain_pre,
    gain_post,
    routes,
    route_weights,
    expert_gate,
    expert_up,
    expert_down,
):
    length = queries_a.shape[0]
    heads_a = queries_a.shape[2] // DA
    heads_b = queries_b.shape[2] // DB
    head_slot = lax.axis_index("tp")
    seq_slot = lax.axis_index("sp")
    lambda_a = lax.dynamic_slice_in_dim(lambdas, head_slot * heads_a, heads_a)
    lambda_b = lax.dynamic_slice_in_dim(lambdas, HA + head_slot * heads_b, heads_b)
    groups = [
        (
            queries_a.reshape(length, 2, heads_a, DA),
            queries_b.reshape(length, 2, heads_b, DB),
            seq_slot * length + jnp.arange(length, dtype=jnp.int32),
            seq_slot * length + length - 1,
        )
    ]
    initial = tuple(
        (
            (
                fresh_state(group[2].shape[0], heads_a, DA),
                fresh_state(group[2].shape[0], heads_b, DB),
            )
            for group in groups
        )
    )
    pieces = (
        lax.all_gather(keys_a, "sp", axis=0, tiled=True),
        lax.all_gather(values_a, "sp", axis=0, tiled=True),
        lax.all_gather(keys_b, "sp", axis=0, tiled=True),
        lax.all_gather(values_b, "sp", axis=0, tiled=True),
    )
    key_count = pieces[0].shape[0]
    span_rows = 1024

    def one_span(span_index, carried):
        offset = span_index * span_rows
        parts = tuple(
            (lax.dynamic_slice_in_dim(piece_part, offset, span_rows, 0) for piece_part in pieces)
        )
        group_qa, group_qb, group_pos, group_last = groups[0]

        def compute(inner, group_qa=group_qa, group_qb=group_qb, group_pos=group_pos):
            return (
                attend(inner[0], group_qa, parts[0], parts[1], offset, group_pos, DA),
                attend(inner[1], group_qb, parts[2], parts[3], offset, group_pos, DB),
            )

        updated = [lax.cond(offset <= group_last, compute, lambda inner: inner, carried[0])]
        return tuple(updated)

    final_state = lax.fori_loop(0, key_count // span_rows, one_span, initial)
    heads_out_a = finish(final_state[0][0], lambda_a, head_gain_a)
    heads_out_b = finish(final_state[0][1], lambda_b, head_gain_b)
    mixed_rows = lax.psum_scatter(
        (
            jnp.dot(heads_out_a, out_a, preferred_element_type=jnp.float32)
            + jnp.dot(heads_out_b, out_b, preferred_element_type=jnp.float32)
        ).astype(jnp.bfloat16),
        "tp",
        scatter_dimension=0,
        tiled=True,
    ).astype(jnp.float32)
    after_mix = (residual.astype(jnp.float32) + rms_norm(mixed_rows, gain_mix)).astype(jnp.bfloat16)
    normed = rms_norm(after_mix.astype(jnp.float32), gain_pre).astype(jnp.bfloat16)
    experts = lax.axis_size("sp")
    sub_rows = residual.shape[0]
    top_count = routes.shape[1]
    capacity = min(sub_rows, (5 * sub_rows * top_count + 4 * experts - 1) // (4 * experts))
    width = residual.shape[1]
    outgoing = jnp.dot(
        send_matrix(routes[None], experts, capacity), normed, preferred_element_type=jnp.float32
    ).astype(jnp.bfloat16)
    outgoing = outgoing.reshape(experts, capacity, width)
    arrived = lax.all_to_all(outgoing, "sp", split_axis=0, concat_axis=0, tiled=True)
    sources, slot_count, columns = arrived.shape
    piece_rows = lax.all_gather(arrived.reshape(-1, columns), "tp", axis=0, tiled=True)
    gate_pre = jnp.dot(piece_rows, expert_gate[0], preferred_element_type=jnp.float32)
    up_pre = jnp.dot(piece_rows, expert_up[0], preferred_element_type=jnp.float32)
    glu_part = jnp.minimum(gate_pre, 7.0)
    lin_part = jnp.clip(up_pre, -7.0, 7.0)
    hidden = (glu_part * jax.nn.sigmoid(1.702 * glu_part) * (lin_part + 1.0)).astype(jnp.bfloat16)
    partials = jnp.dot(hidden, expert_down[0], preferred_element_type=jnp.float32)
    mine = lax.psum_scatter(partials.astype(jnp.bfloat16), "tp", scatter_dimension=0, tiled=True)
    results = mine.reshape(sources, slot_count, columns)
    returned = lax.all_to_all(results, "sp", split_axis=0, concat_axis=0, tiled=True)
    combine = back_matrix(routes, route_weights, experts, capacity)
    routed = jnp.dot(
        combine,
        returned.reshape(-1, width).astype(jnp.float32),
        precision=lax.Precision.HIGHEST,
        preferred_element_type=jnp.float32,
    )
    return (after_mix.astype(jnp.float32) + rms_norm(routed, gain_post)).astype(jnp.bfloat16)


def solution(mesh):
    in_specs = (
        P(("grp", "sp"), None, "tp"),
        P(("grp", "sp"), None, "tp"),
        P(("grp", "sp"), "tp"),
        P(("grp", "sp"), None, "tp"),
        P(("grp", "sp"), None, "tp"),
        P(("grp", "sp"), "tp"),
        P(),
        P(),
        P(),
        P("tp", None),
        P("tp", None),
        P(("grp", "sp", "tp"), None),
        P(),
        P(),
        P(),
        P(("grp", "sp", "tp"), None),
        P(("grp", "sp", "tp"), None),
        P("sp", None, "tp"),
        P("sp", None, "tp"),
        P("sp", "tp", None),
    )
    out_specs = P(("grp", "sp", "tp"), None)
    return jax.shard_map(
        per_device, mesh=mesh, in_specs=in_specs, out_specs=out_specs, check_vma=False
    )
```

profile of v0, /device:TPU:0, one launch (start us, length us, event | category | flops | bytes accessed | tf_op | source)
XLA Modules:
  0.0 503.5 jit_solution(3561112254705816321)
XLA Ops:
  6.6 2.0 copy.36
  8.6 1.8 copy.38
  10.5 1.8 copy.39
  12.4 1.8 copy.41
  17.5 24.9 %all-gather.6.cloned.1.call-done = bf16[2048,2,256]{0,2,1:T(8,128)(2,1)} async-done(((bf16[256,2,256]{0,2,1:T(8,128)(2,1)}), bf16[2048,2,256]{0,2,1:T(8,128)(2,1)}) %all-gather.6.cloned.1.call-update) | async-done | bytes 2097168 | tf_op jit(solution)/shard_map/all_gather | solution.py:149
  42.4 31.3 %all-gather.8.cloned.1.call-done = bf16[2048,512]{0,1:T(8,128)(2,1)} async-done(((bf16[256,512]{0,1:T(8,128)(2,1)}), bf16[2048,512]{0,1:T(8,128)(2,1)}) %all-gather.8.cloned.1.call-update) | async-done | bytes 2097168 | tf_op jit(solution)/shard_map/all_gather | solution.py:150
  73.7 31.3 %all-gather.10.cloned.1.call-done = bf16[2048,2,256]{0,2,1:T(8,128)(2,1)} async-done(((bf16[256,2,256]{0,2,1:T(8,128)(2,1)}), bf16[2048,2,256]{0,2,1:T(8,128)(2,1)}) %all-gather.10.cloned.1.call-update) | async-done | bytes 2097168 | tf_op jit(solution)/shard_map/all_gather | solution.py:151
  104.9 31.1 %all-gather.12.cloned.1.call-done = bf16[2048,512]{0,1:T(8,128)(2,1)} async-done(((bf16[256,512]{0,1:T(8,128)(2,1)}), bf16[2048,512]{0,1:T(8,128)(2,1)}) %all-gather.12.cloned.1.call-update) | async-done | bytes 2097168 | tf_op jit(solution)/shard_map/all_gather | solution.py:152
  137.3 13.8 %while.24 = (s32[]{:T(128)}, f32[2,256,2]{1,2,0:T(2,128)S(1)}, f32[2,256,2]{1,2,0:T(2,128)S(1)}, f32[2,256,2,256]{3,1,0,2:T(8,128)S(1)}, f32[2,256,4]{1,2,0:T(4,...) while((s32[]{:T(128)}, f32[2,256,2]{1,2,0:T(2,128)S(1)}, ...), condition=%wide.region_7.8_spmd.clone, body=%wide.region_0.7_spmd.clone.sunk | while | flops 1640242432 | bytes 83845752 | solution.py:173
  137.3 13.8 %conditional.3 = ((f32[2,256,2]{1,2,0:T(2,128)S(1)}, f32[2,256,2]{1,2,0:T(2,128)S(1)}, f32[2,256,2,256]{3,1,0,2:T(8,128)S(1)}, f32[2,256,4]{1,2,0:T(4,128)S(1)},...) conditional(s32[]{:T(128)} %convert_element_type.151, (f32[2,256,2]{1,2,0:T(2,128)S(1)}, ...), branch_computations={%region_1.0_spmd, %region_2.6_spmd} | conditional | flops 1640242432 | bytes 83844368 | solution.py:170
  137.5 1.8 constant_dynamic-slice_fusion.1
  145.6 2.3 fusion.3
  148.0 2.0 fusion.21
  152.4 2.3 fusion.84
  165.9 29.2 %reduce-scatter.3.cloned.1.call-done = bf16[128,2048]{1,0:T(8,128)(2,1)} async-done(((bf16[256,2048]{1,0:T(8,128)(2,1)}), bf16[128,2048]{1,0:T(8,128)(2,1)}) %reduce-scatter.3.cloned.1.call-update) | async-done | bytes 524304 | tf_op jit(solution)/shard_map/reduce_scatter | solution.py:176
  197.8 3.0 convolution_convert_fusion.1
  200.8 65.0 %all_to_all.10 = bf16[8,80,2048]{2,1,0:T(8,128)(2,1)} all-to-all(bf16[8,80,2048]{2,1,0:T(8,128)(2,1)} %bitcast.199), channel_id=1, replica_groups=mesh['grp'=2,'sp'=8,'tp'=2] {'sp'}, dimensions={0} | all-to-all | bytes 5242880 | tf_op jit(solution)/shard_map/all_to_all | solution.py:196
  265.9 66.6 %all-gather.14.cloned.1.call-done = bf16[1280,2048]{1,0:T(8,128)(2,1)} async-done(((bf16[640,2048]{1,0:T(8,128)(2,1)}), bf16[1280,2048]{1,0:T(8,128)(2,1)}) %all-gather.14.cloned.1.call-update) | async-done | bytes 5242896 | tf_op jit(solution)/shard_map/all_gather | solution.py:198
  332.5 10.2 %fusion.26 = f32[1280,1024]{1,0:T(8,128)} fusion(bf16[1280,2048]{1,0:T(8,128)(2,1)} %all-gather.14.cloned.1.call-done, bf16[1,2048,1024]{2,1,0:T(8,128)(2,1)} %param.41), kind=kOutput, calls=%fused_computation.34 | convolution fusion | flops 5368709120 | bytes 14680064 | tf_op jit(solution)/shard_map/dot_general | solution.py:199
  342.7 18.7 %convolution_convert_fusion = bf16[1280,2048]{1,0:T(8,128)(2,1)} fusion(bf16[1,1024,2048]{2,1,0:T(8,128)(2,1)} %param.43, f32[1280,1024]{1,0:T(8,128)} %fusion.26, bf16[1280,2048]{1,0:T(8,128)(2,1)} %all-gather.14.cloned.1.call-done, bf16[1,2048,1024]{2,1,0:T(8,128)(2,1)} %param.42), kind=kOutput, calls=%fused_computation.30 | convolution fusion | flops 10753146880 | bytes 24117248 | tf_op jit(solution)/shard_map/dot_general | solution.py:204
  361.4 65.9 %reduce-scatter.5.cloned.1.call-done = bf16[640,2048]{1,0:T(8,128)(2,1)} async-done(((bf16[1280,2048]{1,0:T(8,128)(2,1)}), bf16[640,2048]{1,0:T(8,128)(2,1)}) %reduce-scatter.5.cloned.1.call-update) | async-done | bytes 2621456 | tf_op jit(solution)/shard_map/reduce_scatter | solution.py:205
  427.3 4.7 all-to-all-start.1
  433.1 59.3 %all-to-all-done.1 = bf16[8,80,2048]{2,1,0:T(8,128)(2,1)} async-done(((bf16[8,80,2048]{2,1,0:T(8,128)(2,1)}), bf16[8,80,2048]{2,1,0:T(8,128)(2,1)}, u32[]{:S(2)}, u32[]{:S(2)}) %all-to-all-start.1) | async-done | bytes 2621472 | tf_op jit(solution)/shard_map/all_to_all | solution.py:207
  492.4 3.2 multiply_reduce_fusion
  (125 shorter events, 29.3 us)
Async XLA Ops:
  6.5 152.9 %copy-start = (bf16[512,2048]{1,0:T(8,128)(2,1)S(1)}, bf16[512,2048]{1,0:T(8,128)(2,1)}, u32[]{:S(2)}) copy-start(bf16[512,2048]{1,0:T(8,128)(2,1)} %param.33) | copy-start | bytes 6291460
  6.5 9.7 %copy-start.9 = (bf16[256,2,256]{2,1,0:T(2,128)(2,1)S(1)}, bf16[256,2,256]{2,1,0:T(2,128)(2,1)}, u32[]{:S(2)}) copy-start(bf16[256,2,256]{2,1,0:T(2,128)(2,1)} %param.27) | copy-start | bytes 786436
  6.5 10.6 %copy-start.15 = (f32[256]{0:T(256)S(1)}, f32[256]{0:T(256)}, u32[]{:S(2)}) copy-start(f32[256]{0:T(256)} %param.31) | copy-start | bytes 3076
  6.5 10.6 %copy-start.17 = (f32[12]{0:T(128)S(1)}, f32[12]{0:T(128)}, u32[]{:S(2)}) copy-start(f32[12]{0:T(128)} %param.30) | copy-start | bytes 148
  6.5 10.8 %copy-start.16 = (f32[128]{0:T(128)S(1)}, f32[128]{0:T(128)}, u32[]{:S(2)}) copy-start(f32[128]{0:T(128)} %param.32) | copy-start | bytes 1540
  6.5 35.8 %all-gather.6.cloned.1.call-start = ((), (), s32[]{:S(2)}) async-start(), calls=%async_computation.4 | async-start | bytes 2359296 | tf_op jit(solution)/shard_map/all_gather | solution.py:149
  8.6 65.1 %all-gather.8.cloned.1.call-start = ((), (), s32[]{:S(2)}) async-start(), calls=%async_computation.5 | async-start | bytes 2359296 | tf_op jit(solution)/shard_map/all_gather | solution.py:150
  10.5 94.5 %all-gather.10.cloned.1.call-start = ((), (), s32[]{:S(2)}) async-start(), calls=%async_computation.6 | async-start | bytes 2359296 | tf_op jit(solution)/shard_map/all_gather | solution.py:151
  12.4 123.7 %all-gather.12.cloned.1.call-start = ((), (), s32[]{:S(2)}) async-start(), calls=%async_computation.7 | async-start | bytes 2359296 | tf_op jit(solution)/shard_map/all_gather | solution.py:152
  14.3 180.8 %reduce-scatter.3.cloned.1.call-start = ((), (), s32[]{:S(2)}) async-start(), calls=%async_computation.8 | async-start | bytes 1572864 | tf_op jit(solution)/shard_map/reduce_scatter | solution.py:176
  137.5 1.8 copy-start.3
  140.3 1.6 copy-start.1
  140.3 2.2 copy-start.2
  145.6 2.4 copy-start.5
  157.7 2.7 copy-start.7
  160.2 2.0 copy-start.13
  160.2 36.2 %copy-start.8 = (bf16[128,2048]{1,0:T(8,128)(2,1)S(1)}, bf16[128,2048]{1,0:T(8,128)(2,1)}, u32[]{:S(2)}) copy-start(bf16[128,2048]{1,0:T(8,128)(2,1)} %param.35) | copy-start | bytes 1572868
  160.2 36.2 %copy-start.10 = (f32[2048]{0:T(1024)S(1)}, f32[2048]{0:T(1024)}, u32[]{:S(2)}) copy-start(f32[2048]{0:T(1024)} %param.36) | copy-start | bytes 24580
  160.4 37.4 %copy-start.11 = (f32[2048]{0:T(1024)S(1)}, f32[2048]{0:T(1024)}, u32[]{:S(2)}) copy-start(f32[2048]{0:T(1024)} %param.37) | copy-start | bytes 24580
  162.2 170.3 %all-gather.14.cloned.1.call-start = ((), (), s32[]{:S(2)}) async-start(), calls=%async_computation.9 | async-start | bytes 7864320 | tf_op jit(solution)/shard_map/all_gather | solution.py:198
  265.8 161.5 %reduce-scatter.5.cloned.1.call-start = ((), (), s32[]{:S(2)}) async-start(), calls=%async_computation.10 | async-start | bytes 7864320 | tf_op jit(solution)/shard_map/reduce_scatter | solution.py:205
  361.4 70.7 %copy-start.14 = (f32[128,4]{0,1:T(4,128)S(1)}, f32[128,4]{0,1:T(4,128)}, u32[]{:S(2)}) copy-start(f32[128,4]{0,1:T(4,128)} %param.40) | copy-start | bytes 6148
  427.3 68.3 %copy-start.12 = (f32[2048]{0:T(1024)S(1)}, f32[2048]{0:T(1024)}, u32[]{:S(2)}) copy-start(f32[2048]{0:T(1024)} %param.38) | copy-start | bytes 24580
  427.3 65.1 %all-to-all-start.1 = ((bf16[8,80,2048]{2,1,0:T(8,128)(2,1)}), bf16[8,80,2048]{2,1,0:T(8,128)(2,1)}, u32[]{:S(2)}, u32[]{:S(2)}) async-start(bf16[8,80,2048]{2,1,0:T(8,128)(2,1)} %bitcast.202), calls=%async_computation.3 | async-start | bytes 5242880 | tf_op jit(solution)/shard_map/all_to_all | solution.py:207
  (2 other events, 2.6 us)
Sparse Core Ops, SparseCore 0:
  8.9 33.3 all-gather.5
  44.0 29.6 all-gather.7
  75.3 29.6 all-gather.9
  106.4 29.6 all-gather.11
  162.3 32.7 reduce-scatter.2
  266.0 66.4 all-gather.13
  361.5 65.7 reduce-scatter.4
where the time goes:
time: 504 us
  waiting for transfers between devices  340 us (67%)
  blocking collectives  65 us (13%)
  matrix products  44.2 us (9%)
  local copies, waits for them, and re-layouts  22.1 us (4%)
  between operations  13.8 us (3%)
  other arithmetic  13.5 us (3%)
  starting transfers between devices  5.04 us (1%)
    all_gather x1, waiting for transfers between devices, per_device(): lax.all_gather(arrived.reshape(-1, columns), 'tp', axis=0, tiled=True)  66.6 us
    reduce_scatter x1, waiting for transfers between devices, per_device(): lax.psum_scatter(partials.astype(jnp.bfloat16), 'tp', scatter_dimension=0...  65.9 us
    all_to_all x1, blocking collectives, per_device(): lax.all_to_all(outgoing, 'sp', split_axis=0, concat_axis=0, tiled=True)  65 us
    all_to_all x1, waiting for transfers between devices, per_device(): lax.all_to_all(results, 'sp', split_axis=0, concat_axis=0, tiled=True)  59.3 us
    all_gather x1, waiting for transfers between devices, per_device(): lax.all_gather(values_a, 'sp', axis=0, tiled=True)  31.3 us
    all_gather x1, waiting for transfers between devices, per_device(): lax.all_gather(keys_b, 'sp', axis=0, tiled=True)  31.3 us
    all_gather x1, waiting for transfers between devices, per_device(): lax.all_gather(values_b, 'sp', axis=0, tiled=True)  31.1 us
    reduce_scatter x1, waiting for transfers between devices, per_device(): lax.psum_scatter((jnp.dot(heads_out_a, out_a, preferred_element_type=jnp....  29.2 us
  transfers between devices with their start and end apart: 8, of which 8 were waited for; matrix products, arithmetic and copies ran while one was open for 3% of the time, Pallas kernels for 0%

commit v1 on v0

--- a/solution.py
+++ b/solution.py
@@ -6,6 +6,19 @@
 HA = 4
 DA = 128
 DB = 64
+
+
+def ring_gather(x, axis, dim):
+    size, here, rows = (lax.axis_size(axis), lax.axis_index(axis), x.shape[dim])
+    forward = [(i, (i + 1) % size) for i in range(size)]
+    out = jnp.zeros((*x.shape[:dim], size * rows, *x.shape[dim + 1 :]), x.dtype)
+    block = x
+    for step in range(size):
+        source = (here - step) % size
+        out = lax.dynamic_update_slice_in_dim(out, block, source * rows, axis=dim)
+        if step < size - 1:
+            block = lax.ppermute(block, axis, forward)
+    return out
 
 
 def rms_norm(values, gain_vec):
@@ -148,7 +161,7 @@
     pieces = (
         lax.all_gather(keys_a, "sp", axis=0, tiled=True),
         lax.all_gather(values_a, "sp", axis=0, tiled=True),
-        lax.all_gather(keys_b, "sp", axis=0, tiled=True),
+        ring_gather(keys_b, "sp", 0),
         lax.all_gather(values_b, "sp", axis=0, tiled=True),
     )
     key_count = pieces[0].shape[0]

time: 504 us -> 483 us (0.958)
  waiting for transfers between devices: 340 us -> 307 us
  local copies, waits for them, and re-layouts: 22.1 us -> 32.2 us
    ppermute x0 -> x7, waiting for transfers between devices: none -> 60 us  [ring_gather(): block = lax.ppermute(block, axis, forward)]
    all_gather x1, waiting for transfers between devices: 31.3 us -> 0.01 us  [per_device(): lax.all_gather(values_a, 'sp', axis=0, tiled=True)]
    all_gather x1 -> x0, waiting for transfers between devices: 31.3 us -> none  [per_device(): lax.all_gather(keys_b, 'sp', axis=0, tiled=True)]
    all_gather x1, waiting for transfers between devices: 24.9 us -> 0.01 us  [per_device(): lax.all_gather(keys_a, 'sp', axis=0, tiled=True)]
    dynamic_update_slice x0 -> x8, local copies, waits for them, and re-layouts: none -> 6.96 us  [ring_gather(): out = lax.dynamic_update_slice_in_dim(out, block, source * rows, axis=dim)]
    unnamed x37 -> x33, local copies, waits for them, and re-layouts: 10.6 us -> 11.4 us
  transfers between devices with their start and end apart: 8 -> 14, of which waited for: 8 -> 12; matrix products, arithmetic and copies ran while one was open for 3% -> 5% of each run, Pallas kernels for 0% -> 0%
where the time goes in v1:
time: 483 us; the launch traced here: 482 us
  waiting for transfers between devices  307 us (64%)
  blocking collectives  65 us (13%)
  matrix products  44.2 us (9%)
  local copies, waits for them, and re-layouts  32.2 us (7%)
  between operations  13.7 us (3%)
  other arithmetic  13.4 us (3%)
  starting transfers between devices  5.78 us (1%)
    all_gather x1, waiting for transfers between devices, per_device(): lax.all_gather(arrived.reshape(-1, columns), 'tp', axis=0, tiled=True)  66.6 us
    reduce_scatter x1, waiting for transfers between devices, per_device(): lax.psum_scatter(partials.astype(jnp.bfloat16), 'tp', scatter_dimension=0...  65.9 us
    all_to_all x1, blocking collectives, per_device(): lax.all_to_all(outgoing, 'sp', split_axis=0, concat_axis=0, tiled=True)  65 us
    ppermute x7, waiting for transfers between devices, ring_gather(): block = lax.ppermute(block, axis, forward)  60 us
    all_to_all x1, waiting for transfers between devices, per_device(): lax.all_to_all(results, 'sp', split_axis=0, concat_axis=0, tiled=True)  59.3 us
    reduce_scatter x1, waiting for transfers between devices, per_device(): lax.psum_scatter((jnp.dot(heads_out_a, out_a, preferred_element_type=jnp....  29.2 us
    all_gather x1, waiting for transfers between devices, per_device(): lax.all_gather(values_b, 'sp', axis=0, tiled=True)  26.2 us
    dot_general x1, matrix products, per_device(): jnp.dot(hidden, expert_down[0], preferred_element_type=jnp.float32)  18.7 us
  transfers between devices with their start and end apart: 14, of which 12 were waited for; matrix products, arithmetic and copies ran while one was open for 5% of the time, Pallas kernels for 0%

profile of v1, /device:TPU:0, one launch (start us, length us, event | category | flops | bytes accessed | tf_op | source)
XLA Modules:
  0.0 481.8 jit_solution(8793037957856792346)
XLA Ops:
  6.5 2.0 copy.37
  14.0 8.1 %collective-permute-done = bf16[256,2,256]{0,2,1:T(8,128)(2,1)S(1)} collective-permute-done((bf16[256,2,256]{0,2,1:T(8,128)(2,1)S(1)}, bf16[256,2,256]{0,2,1:T(8,128)(2,1)S(1)}, u32[]{:S(2)}, u32[]{:S(2)}) %collective-permute-start) | collective-permute-done | bytes 262176 | tf_op jit(solution)/shard_map/ppermute | solution.py:20
  22.1 12.9 %collective-permute-done.1 = bf16[256,2,256]{0,2,1:T(8,128)(2,1)S(1)} collective-permute-done((bf16[256,2,256]{0,2,1:T(8,128)(2,1)S(1)}, bf16[256,2,256]{0,2,1:T(8,128)(2,1)S(1)}, u32[]{:S(2)}, u32[]{:S(2)}) %collective-permute-start.1) | collective-permute-done | bytes 262176 | tf_op jit(solution)/shard_map/ppermute | solution.py:20
  35.8 10.4 %collective-permute-done.2 = bf16[256,2,256]{0,2,1:T(8,128)(2,1)S(1)} collective-permute-done((bf16[256,2,256]{0,2,1:T(8,128)(2,1)S(1)}, bf16[256,2,256]{0,2,1:T(8,128)(2,1)S(1)}, u32[]{:S(2)}, u32[]{:S(2)}) %collective-permute-start.2) | collective-permute-done | bytes 262176 | tf_op jit(solution)/shard_map/ppermute | solution.py:20
  47.0 6.8 %collective-permute-done.3 = bf16[256,2,256]{0,2,1:T(8,128)(2,1)S(1)} collective-permute-done((bf16[256,2,256]{0,2,1:T(8,128)(2,1)S(1)}, bf16[256,2,256]{0,2,1:T(8,128)(2,1)S(1)}, u32[]{:S(2)}, u32[]{:S(2)}) %collective-permute-start.3) | collective-permute-done | bytes 262176 | tf_op jit(solution)/shard_map/ppermute | solution.py:20
  60.1 6.0 %collective-permute-done.4 = bf16[256,2,256]{0,2,1:T(8,128)(2,1)} collective-permute-done((bf16[256,2,256]{0,2,1:T(8,128)(2,1)S(1)}, bf16[256,2,256]{0,2,1:T(8,128)(2,1)}, u32[]{:S(2)}, u32[]{:S(2)}) %collective-permute-start.4) | collective-permute-done | bytes 262176 | tf_op jit(solution)/shard_map/ppermute | solution.py:20
  68.3 11.3 %collective-permute-done.5 = bf16[256,2,256]{0,2,1:T(8,128)(2,1)S(1)} collective-permute-done((bf16[256,2,256]{0,2,1:T(8,128)(2,1)}, bf16[256,2,256]{0,2,1:T(8,128)(2,1)S(1)}, u32[]{:S(2)}, u32[]{:S(2)}) %collective-permute-start.5) | collective-permute-done | bytes 262176 | tf_op jit(solution)/shard_map/ppermute | solution.py:20
  82.8 4.4 collective-permute-done.6
  88.0 26.2 %all-gather.9.cloned.1.call-done = bf16[2048,512]{0,1:T(8,128)(2,1)} async-done(((bf16[256,512]{0,1:T(8,128)(2,1)}), bf16[2048,512]{0,1:T(8,128)(2,1)}) %all-gather.9.cloned.1.call-update) | async-done | bytes 2097168 | tf_op jit(solution)/shard_map/all_gather | solution.py:165
  115.5 13.8 %while.24 = (s32[]{:T(128)}, f32[2,256,2]{1,2,0:T(2,128)S(1)}, f32[2,256,2]{1,2,0:T(2,128)S(1)}, f32[2,256,2,256]{3,1,0,2:T(8,128)S(1)}, f32[2,256,4]{1,2,0:T(4,...) while((s32[]{:T(128)}, f32[2,256,2]{1,2,0:T(2,128)S(1)}, ...), condition=%wide.region_7.8_spmd.clone, body=%wide.region_0.7_spmd.clone.sunk | while | flops 1640242432 | bytes 83845752 | solution.py:186
  115.5 13.8 %conditional.3 = ((f32[2,256,2]{1,2,0:T(2,128)S(1)}, f32[2,256,2]{1,2,0:T(2,128)S(1)}, f32[2,256,2,256]{3,1,0,2:T(8,128)S(1)}, f32[2,256,4]{1,2,0:T(4,128)S(1)},...) conditional(s32[]{:T(128)} %convert_element_type.151, (f32[2,256,2]{1,2,0:T(2,128)S(1)}, ...), branch_computations={%region_1.1_spmd, %region_2.6_spmd} | conditional | flops 1640242432 | bytes 83844368 | solution.py:183
  123.8 2.3 fusion.3
  126.2 2.0 fusion.21
  130.6 2.3 fusion.84
  144.1 29.2 %reduce-scatter.3.cloned.1.call-done = bf16[128,2048]{1,0:T(8,128)(2,1)} async-done(((bf16[256,2048]{1,0:T(8,128)(2,1)}), bf16[128,2048]{1,0:T(8,128)(2,1)}) %reduce-scatter.3.cloned.1.call-update) | async-done | bytes 524304 | tf_op jit(solution)/shard_map/reduce_scatter | solution.py:189
  176.0 3.0 convolution_convert_fusion.1
  179.0 65.0 %all_to_all.10 = bf16[8,80,2048]{2,1,0:T(8,128)(2,1)} all-to-all(bf16[8,80,2048]{2,1,0:T(8,128)(2,1)} %bitcast.199), channel_id=1, replica_groups=mesh['grp'=2,'sp'=8,'tp'=2] {'sp'}, dimensions={0} | all-to-all | bytes 5242880 | tf_op jit(solution)/shard_map/all_to_all | solution.py:209
  244.1 66.6 %all-gather.11.cloned.1.call-done = bf16[1280,2048]{1,0:T(8,128)(2,1)} async-done(((bf16[640,2048]{1,0:T(8,128)(2,1)}), bf16[1280,2048]{1,0:T(8,128)(2,1)}) %all-gather.11.cloned.1.call-update) | async-done | bytes 5242896 | tf_op jit(solution)/shard_map/all_gather | solution.py:211
  310.7 10.2 %fusion.26 = f32[1280,1024]{1,0:T(8,128)} fusion(bf16[1280,2048]{1,0:T(8,128)(2,1)} %all-gather.11.cloned.1.call-done, bf16[1,2048,1024]{2,1,0:T(8,128)(2,1)} %param.41), kind=kOutput, calls=%fused_computation.34 | convolution fusion | flops 5368709120 | bytes 14680064 | tf_op jit(solution)/shard_map/dot_general | solution.py:212
  320.9 18.7 %convolution_convert_fusion = bf16[1280,2048]{1,0:T(8,128)(2,1)} fusion(bf16[1,1024,2048]{2,1,0:T(8,128)(2,1)} %param.43, f32[1280,1024]{1,0:T(8,128)} %fusion.26, bf16[1280,2048]{1,0:T(8,128)(2,1)} %all-gather.11.cloned.1.call-done, bf16[1,2048,1024]{2,1,0:T(8,128)(2,1)} %param.42), kind=kOutput, calls=%fused_computation.30 | convolution fusion | flops 10753146880 | bytes 24117248 | tf_op jit(solution)/shard_map/dot_general | solution.py:217
  339.6 65.9 %reduce-scatter.5.cloned.1.call-done = bf16[640,2048]{1,0:T(8,128)(2,1)} async-done(((bf16[1280,2048]{1,0:T(8,128)(2,1)}), bf16[640,2048]{1,0:T(8,128)(2,1)}) %reduce-scatter.5.cloned.1.call-update) | async-done | bytes 2621456 | tf_op jit(solution)/shard_map/reduce_scatter | solution.py:218
  405.6 4.8 all-to-all-start.1
  411.4 59.3 %all-to-all-done.1 = bf16[8,80,2048]{2,1,0:T(8,128)(2,1)} async-done(((bf16[8,80,2048]{2,1,0:T(8,128)(2,1)}), bf16[8,80,2048]{2,1,0:T(8,128)(2,1)}, u32[]{:S(2)}, u32[]{:S(2)}) %all-to-all-start.1) | async-done | bytes 2621472 | tf_op jit(solution)/shard_map/all_to_all | solution.py:220
  470.7 3.2 multiply_reduce_fusion
  (141 shorter events, 47.1 us)
Async XLA Ops:
  6.5 131.1 %copy-start = (bf16[512,2048]{1,0:T(8,128)(2,1)S(1)}, bf16[512,2048]{1,0:T(8,128)(2,1)}, u32[]{:S(2)}) copy-start(bf16[512,2048]{1,0:T(8,128)(2,1)} %param.33) | copy-start | bytes 6291460
  6.5 53.4 %copy-start.15 = (f32[12]{0:T(128)S(1)}, f32[12]{0:T(128)}, u32[]{:S(2)}) copy-start(f32[12]{0:T(128)} %param.30) | copy-start | bytes 148
  6.5 53.5 %copy-start.14 = (f32[128]{0:T(128)S(1)}, f32[128]{0:T(128)}, u32[]{:S(2)}) copy-start(f32[128]{0:T(128)} %param.32) | copy-start | bytes 1540
  6.5 81.4 %all-gather.5.cloned.1.call-start = ((), (), s32[]{:S(2)}) async-start(), calls=%async_computation.4 | async-start | bytes 2359296 | tf_op jit(solution)/shard_map/all_gather | solution.py:162
  8.5 79.4 %all-gather.7.cloned.1.call-start = ((), (), s32[]{:S(2)}) async-start(), calls=%async_computation.5 | async-start | bytes 2359296 | tf_op jit(solution)/shard_map/all_gather | solution.py:163
  10.4 103.8 %all-gather.9.cloned.1.call-start = ((), (), s32[]{:S(2)}) async-start(), calls=%async_computation.6 | async-start | bytes 2359296 | tf_op jit(solution)/shard_map/all_gather | solution.py:165
  12.3 161.0 %reduce-scatter.3.cloned.1.call-start = ((), (), s32[]{:S(2)}) async-start(), calls=%async_computation.7 | async-start | bytes 1572864 | tf_op jit(solution)/shard_map/reduce_scatter | solution.py:189
  13.5 8.6 %collective-permute-start = (bf16[256,2,256]{0,2,1:T(8,128)(2,1)S(1)}, bf16[256,2,256]{0,2,1:T(8,128)(2,1)S(1)}, u32[]{:S(2)}, u32[]{:S(2)}) collective-permute-start(bf16[256,2,256]{0,2,1:T(8,128)(2,1)S(1)} %copy.40), channel_id=1, source_target_pairs={{0,2},{2,4},{4,6},{6,8},{8,10},{10,12},{12,14},{14,0},{1,3},{3,5},... | collective-permute-start | bytes 786440 | tf_op jit(solution)/shard_map/ppermute | solution.py:20
  22.1 12.9 %collective-permute-start.1 = (bf16[256,2,256]{0,2,1:T(8,128)(2,1)S(1)}, bf16[256,2,256]{0,2,1:T(8,128)(2,1)S(1)}, u32[]{:S(2)}, u32[]{:S(2)}) collective-permute-start(bf16[256,2,256]{0,2,1:T(8,128)(2,1)S(1)} %collective-permute-done), channel_id=1, source_target_pairs={{0,2},{2,4},{4,6},{6,8},{8,10},{10,12},{12,14},{14,0},{1,3},{3,5},... | collective-permute-start | bytes 786440 | tf_op jit(solution)/shard_map/ppermute | solution.py:20
  35.1 11.2 %collective-permute-start.2 = (bf16[256,2,256]{0,2,1:T(8,128)(2,1)S(1)}, bf16[256,2,256]{0,2,1:T(8,128)(2,1)S(1)}, u32[]{:S(2)}, u32[]{:S(2)}) collective-permute-start(bf16[256,2,256]{0,2,1:T(8,128)(2,1)S(1)} %collective-permute-done.1), channel_id=1, source_target_pairs={{0,2},{2,4},{4,6},{6,8},{8,10},{10,12},{12,14},{14,0},{1,3},{3,5},... | collective-permute-start | bytes 786440 | tf_op jit(solution)/shard_map/ppermute | solution.py:20
  46.2 7.6 %collective-permute-start.3 = (bf16[256,2,256]{0,2,1:T(8,128)(2,1)S(1)}, bf16[256,2,256]{0,2,1:T(8,128)(2,1)S(1)}, u32[]{:S(2)}, u32[]{:S(2)}) collective-permute-start(bf16[256,2,256]{0,2,1:T(8,128)(2,1)S(1)} %collective-permute-done.2), channel_id=1, source_target_pairs={{0,2},{2,4},{4,6},{6,8},{8,10},{10,12},{12,14},{14,0},{1,3},{3,5},... | collective-permute-start | bytes 786440 | tf_op jit(solution)/shard_map/ppermute | solution.py:20
  53.8 12.3 %collective-permute-start.4 = (bf16[256,2,256]{0,2,1:T(8,128)(2,1)S(1)}, bf16[256,2,256]{0,2,1:T(8,128)(2,1)}, u32[]{:S(2)}, u32[]{:S(2)}) collective-permute-start(bf16[256,2,256]{0,2,1:T(8,128)(2,1)S(1)} %collective-permute-done.3), channel_id=1, source_target_pairs={{0,2},{2,4},{4,6},{6,8},{8,10},{10,12},{12,14},{14,0},{1,3},{3,5},... | collective-permute-start | bytes 786440 | tf_op jit(solution)/shard_map/ppermute | solution.py:20
  66.1 13.6 %collective-permute-start.5 = (bf16[256,2,256]{0,2,1:T(8,128)(2,1)}, bf16[256,2,256]{0,2,1:T(8,128)(2,1)S(1)}, u32[]{:S(2)}, u32[]{:S(2)}) collective-permute-start(bf16[256,2,256]{0,2,1:T(8,128)(2,1)} %collective-permute-done.4), channel_id=1, source_target_pairs={{0,2},{2,4},{4,6},{6,8},{8,10},{10,12},{12,14},{14,0},{1,3},{3,5},... | collective-permute-start | bytes 786440 | tf_op jit(solution)/shard_map/ppermute | solution.py:20
  79.6 7.6 %collective-permute-start.6 = (bf16[256,2,256]{0,2,1:T(8,128)(2,1)S(1)}, bf16[256,2,256]{0,2,1:T(8,128)(2,1)S(1)}, u32[]{:S(2)}, u32[]{:S(2)}) collective-permute-start(bf16[256,2,256]{0,2,1:T(8,128)(2,1)S(1)} %collective-permute-done.5), channel_id=1, source_target_pairs={{0,2},{2,4},{4,6},{6,8},{8,10},{10,12},{12,14},{14,0},{1,3},{3,5},... | collective-permute-start | bytes 786440 | tf_op jit(solution)/shard_map/ppermute | solution.py:20
  123.8 2.4 copy-start.5
  135.9 2.7 copy-start.7
  138.4 36.2 %copy-start.8 = (bf16[128,2048]{1,0:T(8,128)(2,1)S(1)}, bf16[128,2048]{1,0:T(8,128)(2,1)}, u32[]{:S(2)}) copy-start(bf16[128,2048]{1,0:T(8,128)(2,1)} %param.35) | copy-start | bytes 1572868
  138.4 36.2 %copy-start.9 = (f32[2048]{0:T(1024)S(1)}, f32[2048]{0:T(1024)}, u32[]{:S(2)}) copy-start(f32[2048]{0:T(1024)} %param.36) | copy-start | bytes 24580
  138.6 37.4 %copy-start.10 = (f32[2048]{0:T(1024)S(1)}, f32[2048]{0:T(1024)}, u32[]{:S(2)}) copy-start(f32[2048]{0:T(1024)} %param.37) | copy-start | bytes 24580
  140.3 170.4 %all-gather.11.cloned.1.call-start = ((), (), s32[]{:S(2)}) async-start(), calls=%async_computation.8 | async-start | bytes 7864320 | tf_op jit(solution)/shard_map/all_gather | solution.py:211
  244.0 161.5 %reduce-scatter.5.cloned.1.call-start = ((), (), s32[]{:S(2)}) async-start(), calls=%async_computation.9 | async-start | bytes 7864320 | tf_op jit(solution)/shard_map/reduce_scatter | solution.py:218
  339.6 70.8 %copy-start.13 = (f32[128,4]{0,1:T(4,128)S(1)}, f32[128,4]{0,1:T(4,128)}, u32[]{:S(2)}) copy-start(f32[128,4]{0,1:T(4,128)} %param.40) | copy-start | bytes 6148
  405.6 68.4 %copy-start.11 = (f32[2048]{0:T(1024)S(1)}, f32[2048]{0:T(1024)}, u32[]{:S(2)}) copy-start(f32[2048]{0:T(1024)} %param.38) | copy-start | bytes 24580
  405.6 65.1 %all-to-all-start.1 = ((bf16[8,80,2048]{2,1,0:T(8,128)(2,1)}), bf16[8,80,2048]{2,1,0:T(8,128)(2,1)}, u32[]{:S(2)}, u32[]{:S(2)}) async-start(bf16[8,80,2048]{2,1,0:T(8,128)(2,1)} %bitcast.202), calls=%async_computation.3 | async-start | bytes 5242880 | tf_op jit(solution)/shard_map/all_to_all | solution.py:220
  (6 other events, 10.5 us)
Sparse Core Ops, SparseCore 0:
  8.9 38.1 all-gather.4
  48.7 33.9 all-gather.6
  84.3 29.8 all-gather.8
  140.5 32.7 reduce-scatter.2
  244.2 66.5 all-gather.10
  339.8 65.7 reduce-scatter.4
